TPU v7x, 32 devices: a whole 2x2x4 slice. The times are simulated.
32 devices in a mesh: sp: 16 (over z, y, core), tp: 2 (over x).
Axes of the slice: x: 2, y: 2, z: 4, core: 2. Of those that a mesh axis runs over, the one named last changes fastest.
Arguments:
- layer_source_rows: bfloat16 [6144, 2048], P(('sp', 'tp')), may hold values from -6 to 6
- entry_rescale_factor: bfloat16 [2048], replicated, may hold values from 0.099609375 to 1.8984375
- sliding_mixer_entry_matrix: bfloat16 [3, 2048, 1024], P(None, 'sp', 'tp'), may hold values from -0.125 to 0.125
- recurrent_mixer_entry_matrix: bfloat16 [2, 2048, 1024], P(None, 'sp', 'tp'), may hold values from -0.125 to 0.125
- latent_write_read_matrix: bfloat16 [2, 2048, 2048], P(None, 'sp', 'tp'), may hold values from -0.125 to 0.125
- timestep_matrix: bfloat16 [2048, 2, 16], P(None, None, 'tp'), may hold values from -0.125 to 0.125
- sliding_kernel_coefficients: bfloat16 [3, 1024], P(None, 'tp'), may hold values from -3.5 to 3.5
- recurrent_kernel_coefficients: bfloat16 [5, 1024], P(None, 'tp'), may hold values from -0.5 to 0.5
- latent_kernel_coefficients: bfloat16 [5, 2, 2048], P(None, None, 'tp'), may hold values from -0.5 to 0.5
- lane_forgetting_rate: float32 [2, 16], P(None, 'tp'), may hold values from 0 to 1
- spike_forgetting_rate: float32 [6144, 16], P('sp', 'tp'), may hold values from -2 to 0
- lane_rescale_factor: bfloat16 [1024], P('tp'), may hold values from 0.099609375 to 1.8984375
- sliding_mixer_exit_matrix: bfloat16 [1024, 2048], P('tp', 'sp'), may hold values from -0.125 to 0.125
- recurrent_mixer_exit_matrix: bfloat16 [1024, 2048], P('tp', 'sp'), may hold values from -0.125 to 0.125
Outputs:
- mixed_out: bfloat16 [6144, 2048], P(('sp', 'tp'))
All inputs are finite; a program needn't handle non-finite values.
Results may differ from a plain program's by a relative error of at most 0.017.
Values may be sent and summed in bfloat16 or wider, within the bound.
No kernel may reach another device: no remote copies, remote signals or barrier semaphores. Data moves between devices by JAX's collectives and lax.ppermute only.
A program may use at most 64 MiB of HBM per device.

v0:
```python
import jax
import jax.numpy as jnp
from jax import lax
from jax.sharding import PartitionSpec as P

HEAD_DIM = 64
STATE = 128
BLOCK = 128
HALO = 8
epsilon = 1e-05


def swapped(value, axis, distance):
    size = lax.axis_size(axis)
    return lax.ppermute(value, axis, [(i, i ^ distance) for i in range(size)])


def tp_rows(normed):
    if lax.axis_size("tp") != 2:
        return lax.all_gather(normed, "tp", axis=0, tiled=True)
    mine = lax.axis_index("tp")
    count = normed.shape[0]
    other = swapped(normed, "tp", 1)
    rows = jnp.zeros((2 * count, normed.shape[1]), normed.dtype)
    rows = lax.dynamic_update_slice(rows, normed, (mine * count, 0))
    return lax.dynamic_update_slice(rows, other, ((1 - mine) * count, 0))


def with_halo(rows):
    size = lax.axis_size("sp")
    up = [(i, i + 1) for i in range(size - 1)]
    down = [(i + 1, i) for i in range(size - 1)]
    before = lax.ppermute(rows[-HALO:], "sp", up)
    after = lax.ppermute(rows[:HALO], "sp", down)
    return jnp.concatenate([before, rows, after], axis=0)


def apply_taps(padded, tap_table, length):
    taps = tap_table.shape[0]
    first = HALO - taps // 2
    summed = jnp.zeros((length, padded.shape[1]), jnp.float32)
    for offset in range(taps):
        summed = summed + padded[first + offset : first + offset + length].astype(
            jnp.float32
        ) * tap_table[offset].astype(jnp.float32)
    return summed


def decay_levels(decay):
    place = lax.axis_index("sp")
    levels = []
    ahead = jnp.ones_like(decay)
    distance = 1
    while distance < lax.axis_size("sp"):
        other = swapped(decay, "sp", distance)
        upper = place & distance != 0
        joins = jnp.stack([upper, ~upper])
        levels.append((distance, joins[:, None], decay, other, ahead))
        ahead = jnp.where(joins[:, None], ahead * other, ahead)
        decay = decay * other
        distance *= 2
    return levels


def entering_state(total, levels):
    place = lax.axis_index("sp")
    prefix = jnp.zeros_like(total)
    for number, (distance, joins, own, other, ahead) in enumerate(levels):
        wide = lambda a: a[..., None, None]
        joins = joins[None, :, :, None]
        if number + 1 < len(levels):
            got = swapped(total.astype(jnp.bfloat16), "sp", distance).astype(jnp.float32)
            prefix = jnp.where(joins, got * wide(ahead) + prefix, prefix)
            total = jnp.where(joins, got * wide(own) + total, total * wide(other) + got)
        else:
            upper = place & distance != 0
            send = jnp.where(upper, total[:, 1], total[:, 0]).astype(jnp.bfloat16)
            got = swapped(send, "sp", distance).astype(jnp.float32)
            prefix = jnp.where(joins, got[:, None] * wide(ahead) + prefix, prefix)
    return prefix


def local(
    layer_source_rows,
    entry_rescale_factor,
    sliding_mixer_entry_matrix,
    recurrent_mixer_entry_matrix,
    latent_write_read_matrix,
    timestep_matrix,
    sliding_kernel_coefficients,
    recurrent_kernel_coefficients,
    latent_kernel_coefficients,
    lane_forgetting_rate,
    spike_forgetting_rate,
    lane_rescale_factor,
    sliding_mixer_exit_matrix,
    recurrent_mixer_exit_matrix,
):
    f32, bf16 = (jnp.float32, jnp.bfloat16)
    conv_width = sliding_mixer_entry_matrix.shape[2]
    ssd_width = recurrent_mixer_entry_matrix.shape[2]
    state_width = latent_write_read_matrix.shape[2]
    heads = timestep_matrix.shape[2]
    assert state_width == heads * STATE and ssd_width == heads * HEAD_DIM
    ssd_shard = jnp.concatenate(
        [
            recurrent_mixer_entry_matrix[0],
            recurrent_mixer_entry_matrix[1],
            latent_write_read_matrix[0],
            latent_write_read_matrix[1],
        ],
        axis=1,
    )
    ssd_weight = lax.all_gather(ssd_shard, "sp", axis=0, tiled=True)
    float_rows = layer_source_rows.astype(f32)
    normed = (
        float_rows
        * lax.rsqrt(jnp.mean(float_rows * float_rows, axis=-1, keepdims=True) + epsilon)
        * entry_rescale_factor.astype(f32)
    ).astype(bf16)
    rows = tp_rows(normed)
    length = rows.shape[0]
    exit_shard = jnp.concatenate([sliding_mixer_exit_matrix, recurrent_mixer_exit_matrix], axis=0).T
    conv_shard = jnp.concatenate(
        [sliding_mixer_entry_matrix[k] for k in range(3)] + [exit_shard], axis=1
    )
    conv_shard, rows = lax.optimization_barrier((conv_shard, rows))
    conv_weight = lax.all_gather(conv_shard, "sp", axis=0, tiled=True)
    wide_rows = with_halo(rows)
    raw_step = (
        jnp.dot(rows, timestep_matrix.reshape(-1, 2 * heads), preferred_element_type=f32)
        .astype(bf16)
        .astype(f32)
        .reshape(length, 2, heads)
    )
    deltas = jax.nn.softplus(raw_step)
    log_decay = -deltas * lane_forgetting_rate[None] + spike_forgetting_rate[:, None, :]
    blocks = length // BLOCK
    order = jnp.arange(BLOCK)
    lower = (order[:, None] >= order[None, :]).astype(f32)
    sums = jnp.stack([lower, lower.T])
    logs = log_decay.reshape(blocks, BLOCK, 2, heads).transpose(2, 3, 0, 1)
    delta = deltas.reshape(blocks, BLOCK, 2, heads).transpose(2, 3, 0, 1)
    running = jnp.einsum("dhbs,dts->dhbt", logs, sums, precision=lax.Precision.HIGHEST)
    ends = jnp.stack([running[0, :, :, -1], running[1, :, :, 0]])
    to_end = jnp.exp(ends[..., None] - running) * delta
    levels = decay_levels(jnp.exp(jnp.sum(ends, axis=-1)))
    levels = [(n, j, a.T, b.T, c.T) for n, j, a, b, c in levels]
    before_ends = jnp.cumsum(ends[0], axis=-1) - ends[0]
    after_ends = jnp.cumsum(ends[1][:, ::-1], axis=-1)[:, ::-1] - ends[1]
    starts = jnp.exp(jnp.stack([before_ends, after_ends]))
    mask = order[:, None] >= order[None, :]
    gaps = running[..., :, None] - running[..., None, :]
    decays = (
        jnp.where(mask, jnp.exp(jnp.where(mask, gaps[0], 0.0)), 0.0) * delta[0][..., None, :]
        + jnp.where(mask.T, jnp.exp(jnp.where(mask.T, gaps[1], 0.0)), 0.0) * delta[1][..., None, :]
    )
    projected = jnp.dot(wide_rows, ssd_weight, preferred_element_type=f32).astype(bf16)
    ssd_gate = projected[HALO : HALO + length, :ssd_width]
    joined_taps = jnp.concatenate(
        [
            recurrent_kernel_coefficients,
            latent_kernel_coefficients.reshape(latent_kernel_coefficients.shape[0], -1),
        ],
        axis=1,
    )
    mixed = jax.nn.silu(apply_taps(projected[:, ssd_width:], joined_taps, length)).astype(bf16)
    ssd_x = mixed[:, :ssd_width].reshape(blocks, BLOCK, heads, HEAD_DIM)
    keys_b = mixed[:, ssd_width : ssd_width + state_width].reshape(blocks, BLOCK, heads, STATE)
    reads_c = mixed[:, ssd_width + state_width :].reshape(blocks, BLOCK, heads, STATE)
    ssd_x = ssd_x.transpose(2, 0, 1, 3)
    keys_b = keys_b.transpose(2, 0, 1, 3)
    reads_c = reads_c.transpose(2, 0, 1, 3)
    x_float = ssd_x.astype(f32)
    weighted = jnp.concatenate(
        [(x_float * to_end[d][..., None]).astype(bf16) for d in range(2)], axis=-1
    )
    contribution = jnp.einsum("hbsp,hbsn->hbpn", weighted, keys_b, preferred_element_type=f32)
    contribution = contribution.reshape(heads, blocks, 2, HEAD_DIM, STATE)
    end_decay = jnp.exp(ends)[..., None, None]
    forward, fore = ([], jnp.zeros((heads, HEAD_DIM, STATE), f32))
    for b in range(blocks):
        forward.append(fore)
        fore = fore * end_decay[0, :, b] + contribution[:, b, 0]
    backward, aft = ([None] * blocks, jnp.zeros((heads, HEAD_DIM, STATE), f32))
    for b in reversed(range(blocks)):
        backward[b] = aft
        aft = aft * end_decay[1, :, b] + contribution[:, b, 1]
    prefix = entering_state(jnp.stack([fore, aft], axis=1), levels)
    scores = jnp.einsum("hbtn,hbsn->hbts", reads_c, keys_b, preferred_element_type=f32)
    within = jnp.einsum(
        "hbts,hbsp->hbtp", (scores * decays).astype(bf16), ssd_x, preferred_element_type=f32
    )
    inside = jnp.stack([jnp.stack(forward, 1), jnp.stack(backward, 1)], axis=2)
    entering = inside + prefix[:, None] * starts.transpose(1, 2, 0)[..., None, None]
    entering = entering.astype(bf16).reshape(heads, blocks, 2 * HEAD_DIM, STATE)
    carried = jnp.einsum("hbtn,hbpn->hbtp", reads_c, entering, preferred_element_type=f32)
    grown = jnp.exp(running)[..., None]
    y = within + carried[..., :HEAD_DIM] * grown[0] + carried[..., HEAD_DIM:] * grown[1]
    gate = ssd_gate.astype(f32).reshape(blocks, BLOCK, heads, HEAD_DIM).transpose(2, 0, 1, 3)
    y = y * jax.nn.silu(gate)
    y = y * lax.rsqrt(jnp.mean(y * y, axis=-1, keepdims=True) + epsilon)
    y = y * lane_rescale_factor.astype(f32).reshape(heads, 1, 1, HEAD_DIM)
    y_ssd = y.astype(bf16).transpose(1, 2, 0, 3).reshape(length, ssd_width)
    conv = jnp.dot(wide_rows, conv_weight[:, : 3 * conv_width], preferred_element_type=f32).astype(
        bf16
    )
    out_gate = conv[HALO : HALO + length, :conv_width].astype(f32)
    gated_in = (
        conv[:, conv_width : 2 * conv_width].astype(f32) * conv[:, 2 * conv_width :].astype(f32)
    ).astype(bf16)
    y_conv = (out_gate * apply_taps(gated_in, sliding_kernel_coefficients, length)).astype(bf16)
    mixed_y = jnp.concatenate([y_conv, y_ssd], axis=1)
    exit_weight = conv_weight[:, 3 * conv_width :]

    def leave(part):
        return lax.dot_general(
            part, exit_weight, (((1,), (1,)), ((), ())), preferred_element_type=f32
        ).astype(bf16)

    if lax.axis_size("tp") != 2:
        return lax.psum_scatter(leave(mixed_y), "tp", scatter_dimension=0, tiled=True)
    mine = lax.axis_index("tp")
    half = length // 2
    sent = leave(lax.dynamic_slice_in_dim(mixed_y, (1 - mine) * half, half, 0))
    got = swapped(sent, "tp", 1)
    kept = leave(lax.dynamic_slice_in_dim(mixed_y, mine * half, half, 0))
    return (kept.astype(f32) + got.astype(f32)).astype(bf16)


def solution(mesh):
    placed = (
        P(("sp", "tp"), None),
        P(),
        P(None, "sp", "tp"),
        P(None, "sp", "tp"),
        P(None, "sp", "tp"),
        P(None, None, "tp"),
        P(None, "tp"),
        P(None, "tp"),
        P(None, None, "tp"),
        P(None, "tp"),
        P("sp", "tp"),
        P("tp"),
        P("tp", "sp"),
        P("tp", "sp"),
    )
    return jax.shard_map(
        local, mesh=mesh, in_specs=placed, out_specs=P(("sp", "tp"), None), check_vma=False
    )
```

profile of v0, /device:TPU:0, one launch (start us, length us, event | category | flops | bytes accessed | tf_op | source)
XLA Modules:
  0.0 282.8 jit_solution(1260736302038786378)
XLA Ops:
  10.5 3.0 %collective-permute-start = (bf16[192,2048]{1,0:T(8,128)(2,1)S(1)}, bf16[192,2048]{1,0:T(8,128)(2,1)S(1)}, u32[]{:S(2)}, u32[]{:S(2)}) collective-permute-start(bf16[192,2048]{1,0:T(8,128)(2,1)S(1)} %get-tuple-element.25), channel_id=1, source_target_pairs={{0,1},{1,0},{2,3},{3,2},{4,5},{5,4},{6,7},{7,6},{8,9},{9,8},{10,11... | collective-permute-start | bytes 2359304 | tf_op jit(solution)/shard_map/ppermute | solution.py:15
  13.5 1.8 fusion.125
  19.1 1.8 pad_maximum_fusion.2
  21.0 10.1 %collective-permute-done = bf16[192,2048]{1,0:T(8,128)(2,1)S(1)} collective-permute-done((bf16[192,2048]{1,0:T(8,128)(2,1)S(1)}, bf16[192,2048]{1,0:T(8,128)(2,1)S(1)}, u32[]{:S(2)}, u32[]{:S(2)}) %collective-permute-start) | collective-permute-done | bytes 786464 | tf_op jit(solution)/shard_map/ppermute | solution.py:15
  35.4 2.4 collective-permute-start.1
  42.0 2.2 broadcast_subtract_fusion
  44.7 3.6 %collective-permute-start.6 = (f32[2,8]{1,0:T(2,128)S(1)}, f32[2,8]{1,0:T(2,128)S(1)}, u32[]{:S(2)}, u32[]{:S(2)}) collective-permute-start(f32[2,8]{1,0:T(2,128)S(1)} %get-tuple-element.64), channel_id=1, source_target_pairs={{0,4},{2,6},{4,0},{6,2},{8,12},{10,14},{12,8},{14,10},{16,20},{18,... | collective-permute-start | bytes 200 | tf_op jit(solution)/shard_map/ppermute | solution.py:15
  49.9 3.0 %collective-permute-start.8 = (f32[2,8]{1,0:T(2,128)S(1)}, f32[2,8]{1,0:T(2,128)S(1)}, u32[]{:S(2)}, u32[]{:S(2)}) collective-permute-start(f32[2,8]{1,0:T(2,128)S(1)} %mul.523), channel_id=1, source_target_pairs={{0,8},{2,10},{4,12},{6,14},{8,0},{10,2},{12,4},{14,6},{16,24},{18,... | collective-permute-start | bytes 200 | tf_op jit(solution)/shard_map/ppermute | solution.py:15
  59.7 53.7 %all-gather.5.cloned.1.call-done = bf16[2048,3072]{1,0:T(8,128)(2,1)} async-done(((bf16[128,3072]{1,0:T(8,128)(2,1)}), bf16[2048,3072]{1,0:T(8,128)(2,1)}) %all-gather.5.cloned.1.call-update) | async-done | bytes 12582928 | tf_op jit(solution)/shard_map/all_gather | solution.py:114
  113.4 8.7 %convolution_convert_fusion = bf16[400,3072]{1,0:T(8,128)(2,1)S(1)} fusion(bf16[400,2048]{1,0:T(8,128)(2,1)} %constant_dynamic-update-slice_fusion, bf16[2048,3072]{1,0:T(8,128)(2,1)} %all-gather.5.cloned.1.call-done), kind=kOutput, calls=%fused_computation.2 | convolution fusion | flops 5034393600 | bytes 16678912 | tf_op jit(solution)/shard_map/dot_general | solution.py:158
  122.1 4.2 %multiply_convert_fusion = bf16[384,2560]{1,0:T(8,128)(2,1)} fusion(bf16[400,3072]{1,0:T(8,128)(2,1)S(1)} %convolution_convert_fusion, f32[2560]{0:T(1024)S(1)} %get-tuple-element.10, f32[2560]{0:T(1024)S(1)} %get-tuple-element.11, f32[2560]{0:T(1024)S(1)} %get-tuple-element.12, f32[2560]{0:T(1024)S(1)} %get-tuple-element.13, f32[2560]{0:T(1024)S(1)} %get-tuple-element.9), kind=kLoop, calls=%fused_computation.3 | loop fusion | flops 18677760 | bytes 11847680 | tf_op jit(solution)/shard_map/convert_element_type | solution.py:167
  126.3 1.8 slice.271
  128.0 1.7 reshape.312
  131.0 2.4 slice_bitcast_fusion.3
  136.0 68.2 %all-gather.3.cloned.1.call-done = bf16[2048,2560]{0,1:T(8,128)(2,1)} async-done(((bf16[128,2560]{0,1:T(8,128)(2,1)}), bf16[2048,2560]{0,1:T(8,128)(2,1)}) %all-gather.3.cloned.1.call-update) | async-done | bytes 10485776 | tf_op jit(solution)/shard_map/all_gather | solution.py:128
  204.2 6.0 %fusion.6 = bf16[400,1536]{1,0:T(8,128)(2,1)S(1)} fusion(bf16[400,2048]{1,0:T(8,128)(2,1)} %constant_dynamic-update-slice_fusion, bf16[2048,2560]{0,1:T(8,128)(2,1)} %all-gather.3.cloned.1.call-done), kind=kOutput, calls=%fused_computation.8 | convolution fusion | flops 2517196800 | bytes 9158656 | tf_op jit(solution)/shard_map/dot_general | solution.py:205
  213.3 5.8 %collective-permute-done.5 = bf16[8,2,64,128]{3,2,1,0:T(8,128)(2,1)S(1)} collective-permute-done((bf16[8,2,64,128]{3,2,1,0:T(8,128)(2,1)S(1)}, bf16[8,2,64,128]{3,2,1,0:T(8,128)(2,1)S(1)}, u32[]{:S(2)}, u32[]{:S(2)}) %collective-permute-start.5) | collective-permute-done | bytes 262176 | tf_op jit(solution)/shard_map/ppermute | solution.py:15
  225.4 2.8 collective-permute-done.7
  231.4 6.0 %collective-permute-done.9 = bf16[8,64,128]{2,1,0:T(8,128)(2,1)S(1)} collective-permute-done((bf16[8,64,128]{2,1,0:T(8,128)(2,1)S(1)}, bf16[8,64,128]{2,1,0:T(8,128)(2,1)S(1)}, u32[]{:S(2)}, u32[]{:S(2)}) %collective-permute-start.9) | collective-permute-done | bytes 131104 | tf_op jit(solution)/shard_map/ppermute | solution.py:15
  239.8 1.8 fusion.49
  241.7 5.2 %multiply_reduce_fusion = (f32[8,3,128]{2,1,0:T(4,128)}, f32[8,3,128,64]{2,3,1,0:T(8,128)}) fusion(f32[3,128,8,64]{1,3,0,2:T(8,128)} %copy.135, f32[8,3,128]{2,1,0:T(4,128)} %copy.133, f32[8,3,128,128]{2,3,1,0:T(8,128)} %fusion.49, f32[8,3,128]{2,1,0:T(4,128)} %copy.132, bf16[3,128,8,64]{1,3,0,2:T(8,128)(2,1)S(1)} %copy-done.9, ...), kind=kOutput, calls=%fused_computation.73 | convolution fusion | flops 156693504 | bytes 8351744 | tf_op jit(solution)/shard_map/hbts,hbsp->hbtp/dot_general | solution.py:191
  249.9 3.2 %fusion.15 = bf16[192,2048]{1,0:T(8,128)(2,1)S(1)} fusion(bf16[2048,2560]{0,1:T(8,128)(2,1)} %all-gather.3.cloned.1.call-done, s32[]{:T(128)S(6)} %select_n.69, bf16[384,512]{1,0:T(8,128)(2,1)S(1)} %copy-done.13, bf16[384,512]{1,0:T(8,128)(2,1)S(1)} %reshape.314), kind=kOutput, calls=%fused_computation.11 | convolution fusion | flops 806486016 | bytes 5767172 | tf_op jit(solution)/shard_map/dot_general | solution.py:217
  254.6 17.2 %collective-permute-done.10 = bf16[192,2048]{1,0:T(8,128)(2,1)S(1)} collective-permute-done((bf16[192,2048]{1,0:T(8,128)(2,1)S(1)}, bf16[192,2048]{1,0:T(8,128)(2,1)S(1)}, u32[]{:S(2)}, u32[]{:S(2)}) %collective-permute-start.10) | collective-permute-done | bytes 786464 | tf_op jit(solution)/shard_map/ppermute | solution.py:15
  271.8 4.1 %add_convert_fusion = bf16[192,2048]{1,0:T(8,128)(2,1)} fusion(bf16[192,2048]{1,0:T(8,128)(2,1)S(1)} %collective-permute-done.10, bf16[2048,2560]{0,1:T(8,128)(2,1)} %all-gather.3.cloned.1.call-done, s32[]{:T(128)S(6)} %select_n.68, bf16[384,512]{1,0:T(8,128)(2,1)S(1)} %copy-done.13, bf16[384,512]{1,0:T(8,128)(2,1)S(1)} %reshape.314), kind=kOutput, calls=%fused_computation.33 | convolution fusion | flops 808058880 | bytes 6553604 | tf_op jit(solution)/shard_map/dot_general | solution.py:217
  (196 shorter events, 48.0 us)
Async XLA Ops:
  6.5 27.6 %copy-start = (bf16[2048,2,8]{0,2,1:T(8,128)(2,1)S(1)}, bf16[2048,2,8]{0,2,1:T(8,128)(2,1)}, u32[]{:S(2)}) copy-start(bf16[2048,2,8]{0,2,1:T(8,128)(2,1)} %param.19) | copy-start | bytes 196612
  6.5 106.9 %all-gather.5.cloned.1.call-start = ((), (), s32[]{:S(2)}) async-start(), calls=%async_computation.1 | async-start | bytes 13369344 | tf_op jit(solution)/shard_map/all_gather | solution.py:114
  9.7 194.5 %all-gather.3.cloned.1.call-start = ((), (), s32[]{:S(2)}) async-start(), calls=%async_computation | async-start | bytes 11141120 | tf_op jit(solution)/shard_map/all_gather | solution.py:128
  10.5 20.6 %collective-permute-start = (bf16[192,2048]{1,0:T(8,128)(2,1)S(1)}, bf16[192,2048]{1,0:T(8,128)(2,1)S(1)}, u32[]{:S(2)}, u32[]{:S(2)}) collective-permute-start(bf16[192,2048]{1,0:T(8,128)(2,1)S(1)} %get-tuple-element.25), channel_id=1, source_target_pairs={{0,1},{1,0},{2,3},{3,2},{4,5},{5,4},{6,7},{7,6},{8,9},{9,8},{10,11... | collective-permute-start | bytes 2359304 | tf_op jit(solution)/shard_map/ppermute | solution.py:15
  19.1 12.1 %copy-start.14 = (bf16[5,2,1024]{2,1,0:T(2,128)(2,1)S(1)}, bf16[5,2,1024]{2,1,0:T(2,128)(2,1)}, u32[]{:S(2)}) copy-start(bf16[5,2,1024]{2,1,0:T(2,128)(2,1)} %param.22) | copy-start | bytes 61444
  19.1 12.1 %copy-start.35 = (bf16[512]{0:T(512)(128)(2,1)S(1)}, bf16[512]{0:T(512)(128)(2,1)}, u32[]{:S(2)}) copy-start(bf16[512]{0:T(512)(128)(2,1)} %param.25) | copy-start | bytes 3076
  19.1 13.6 %copy-start.29 = (bf16[5,512]{1,0:T(8,128)(2,1)S(1)}, bf16[5,512]{1,0:T(8,128)(2,1)}, u32[]{:S(2)}) copy-start(bf16[5,512]{1,0:T(8,128)(2,1)} %param.21) | copy-start | bytes 15364
  19.1 14.4 %copy-start.23 = (bf16[3,512]{1,0:T(4,128)(2,1)S(1)}, bf16[3,512]{1,0:T(4,128)(2,1)}, u32[]{:S(2)}) copy-start(bf16[3,512]{1,0:T(4,128)(2,1)} %param.20) | copy-start | bytes 9220
  32.0 22.5 %copy-start.21 = (pred[2]{0:T(512)(128)(4,1)}, pred[2]{0:T(512)(128)(4,1)S(1)}, u32[]{:S(2)}) copy-start(pred[2]{0:T(512)(128)(4,1)S(1)} %pad_add_fusion.3) | copy-start | bytes 10
  32.1 22.4 %copy-start.24 = (pred[2]{0:T(512)(128)(4,1)}, pred[2]{0:T(512)(128)(4,1)S(1)}, u32[]{:S(2)}) copy-start(pred[2]{0:T(512)(128)(4,1)S(1)} %pad_add_fusion.2) | copy-start | bytes 10
  32.1 22.3 %copy-start.30 = (pred[2]{0:T(512)(128)(4,1)}, pred[2]{0:T(512)(128)(4,1)S(1)}, u32[]{:S(2)}) copy-start(pred[2]{0:T(512)(128)(4,1)S(1)} %pad_add_fusion.1) | copy-start | bytes 10
  35.2 9.5 %collective-permute-start.4 = (f32[2,8]{1,0:T(2,128)S(1)}, f32[2,8]{1,0:T(2,128)S(1)}, u32[]{:S(2)}, u32[]{:S(2)}) collective-permute-start(f32[2,8]{1,0:T(2,128)S(1)} %exp.52), channel_id=1, source_target_pairs={{0,2},{2,0},{4,6},{6,4},{8,10},{10,8},{12,14},{14,12},{16,18},{18,... | collective-permute-start | bytes 200 | tf_op jit(solution)/shard_map/ppermute | solution.py:15
  35.4 21.8 %collective-permute-start.1 = (bf16[8,2048]{1,0:T(8,128)(2,1)S(1)}, bf16[8,2048]{1,0:T(8,128)(2,1)S(1)}, u32[]{:S(2)}, u32[]{:S(2)}) collective-permute-start(bf16[8,2048]{1,0:T(8,128)(2,1)S(1)} %get-tuple-element.32), channel_id=1, source_target_pairs={{0,2},{2,4},{4,6},{6,8},{8,10},{10,12},{12,14},{14,16},{16,18},{18... | collective-permute-start | bytes 98312 | tf_op jit(solution)/shard_map/ppermute | solution.py:33
  37.8 21.3 %collective-permute-start.2 = (bf16[8,2048]{1,0:T(8,128)(2,1)S(1)}, bf16[8,2048]{1,0:T(8,128)(2,1)S(1)}, u32[]{:S(2)}, u32[]{:S(2)}) collective-permute-start(bf16[8,2048]{1,0:T(8,128)(2,1)S(1)} %get-tuple-element.31), channel_id=1, source_target_pairs={{2,0},{4,2},{6,4},{8,6},{10,8},{12,10},{14,12},{16,14},{18,16},{20... | collective-permute-start | bytes 98312 | tf_op jit(solution)/shard_map/ppermute | solution.py:34
  44.7 5.2 %collective-permute-start.6 = (f32[2,8]{1,0:T(2,128)S(1)}, f32[2,8]{1,0:T(2,128)S(1)}, u32[]{:S(2)}, u32[]{:S(2)}) collective-permute-start(f32[2,8]{1,0:T(2,128)S(1)} %get-tuple-element.64), channel_id=1, source_target_pairs={{0,4},{2,6},{4,0},{6,2},{8,12},{10,14},{12,8},{14,10},{16,20},{18,... | collective-permute-start | bytes 200 | tf_op jit(solution)/shard_map/ppermute | solution.py:15
  49.9 4.5 %collective-permute-start.8 = (f32[2,8]{1,0:T(2,128)S(1)}, f32[2,8]{1,0:T(2,128)S(1)}, u32[]{:S(2)}, u32[]{:S(2)}) collective-permute-start(f32[2,8]{1,0:T(2,128)S(1)} %mul.523), channel_id=1, source_target_pairs={{0,8},{2,10},{4,12},{6,14},{8,0},{10,2},{12,4},{14,6},{16,24},{18,... | collective-permute-start | bytes 200 | tf_op jit(solution)/shard_map/ppermute | solution.py:15
  135.7 74.6 %copy-start.22 = (pred[2]{0:T(512)(128)(4,1)S(1)}, pred[2]{0:T(512)(128)(4,1)}, u32[]{:S(2)}) copy-start(pred[2]{0:T(512)(128)(4,1)} %copy-done.21) | copy-start | bytes 10
  135.7 74.5 %collective-permute-start.3 = (bf16[8,2,64,128]{3,2,1,0:T(8,128)(2,1)S(1)}, bf16[8,2,64,128]{3,2,1,0:T(8,128)(2,1)S(1)}, u32[]{:S(2)}, u32[]{:S(2)}) collective-permute-start(bf16[8,2,64,128]{3,2,1,0:T(8,128)(2,1)S(1)} %fusion.70), channel_id=1, source_target_pairs={{0,2},{2,0},{4,6},{6,4},{8,10},{10,8},{12,14},{14,12},{16,18},{18,... | collective-permute-start | bytes 786440 | tf_op jit(solution)/shard_map/ppermute | solution.py:15
  210.6 8.5 %copy-start.25 = (pred[2]{0:T(512)(128)(4,1)S(1)}, pred[2]{0:T(512)(128)(4,1)}, u32[]{:S(2)}) copy-start(pred[2]{0:T(512)(128)(4,1)} %copy-done.24) | copy-start | bytes 10
  210.6 8.5 %collective-permute-start.5 = (bf16[8,2,64,128]{3,2,1,0:T(8,128)(2,1)S(1)}, bf16[8,2,64,128]{3,2,1,0:T(8,128)(2,1)S(1)}, u32[]{:S(2)}, u32[]{:S(2)}) collective-permute-start(bf16[8,2,64,128]{3,2,1,0:T(8,128)(2,1)S(1)} %fusion.118), channel_id=1, source_target_pairs={{0,4},{2,6},{4,0},{6,2},{8,12},{10,14},{12,8},{14,10},{16,20},{18,... | collective-permute-start | bytes 786440 | tf_op jit(solution)/shard_map/ppermute | solution.py:15
  213.3 7.9 %copy-start.6 = (bf16[48,8,8,128]{3,1,2,0:T(8,128)(2,1)S(1)}, bf16[48,8,8,128]{3,1,2,0:T(8,128)(2,1)}, u32[]{:S(2)}) copy-start(bf16[48,8,8,128]{3,1,2,0:T(8,128)(2,1)} %get-tuple-element.26) | copy-start | bytes 2359300
  220.2 7.9 %collective-permute-start.7 = (bf16[8,2,64,128]{3,2,1,0:T(8,128)(2,1)}, bf16[8,2,64,128]{3,2,1,0:T(8,128)(2,1)}, u32[]{:S(2)}, u32[]{:S(2)}) collective-permute-start(bf16[8,2,64,128]{3,2,1,0:T(8,128)(2,1)} %fusion.90), channel_id=1, source_target_pairs={{0,8},{2,10},{4,12},{6,14},{8,0},{10,2},{12,4},{14,6},{16,24},{18,... | collective-permute-start | bytes 786440 | tf_op jit(solution)/shard_map/ppermute | solution.py:15
  229.6 7.7 %collective-permute-start.9 = (bf16[8,64,128]{2,1,0:T(8,128)(2,1)S(1)}, bf16[8,64,128]{2,1,0:T(8,128)(2,1)S(1)}, u32[]{:S(2)}, u32[]{:S(2)}) collective-permute-start(bf16[8,64,128]{2,1,0:T(8,128)(2,1)S(1)} %fusion.88), channel_id=1, source_target_pairs={{0,16},{2,18},{4,20},{6,22},{8,24},{10,26},{12,28},{14,30},{16,0},... | collective-permute-start | bytes 393224 | tf_op jit(solution)/shard_map/ppermute | solution.py:15
  253.1 18.8 %collective-permute-start.10 = (bf16[192,2048]{1,0:T(8,128)(2,1)S(1)}, bf16[192,2048]{1,0:T(8,128)(2,1)S(1)}, u32[]{:S(2)}, u32[]{:S(2)}) collective-permute-start(bf16[192,2048]{1,0:T(8,128)(2,1)S(1)} %fusion.15), channel_id=1, source_target_pairs={{0,1},{1,0},{2,3},{3,2},{4,5},{5,4},{6,7},{7,6},{8,9},{9,8},{10,11... | collective-permute-start | bytes 2359304 | tf_op jit(solution)/shard_map/ppermute | solution.py:15
  (28 other events, 83.3 us)
Sparse Core Ops, SparseCore 0:
  9.8 103.5 all-gather.4
  115.5 88.5 all-gather.2
where the time goes:
time: 283 us
  waiting for transfers between devices  166 us (59%)
  matrix products  30.1 us (11%)
  local copies, waits for them, and re-layouts  29 us (10%)
  other arithmetic  25.2 us (9%)
  starting transfers between devices  18.4 us (7%)
  between operations  14.2 us (5%)
    all_gather x1, waiting for transfers between devices, local(): conv_weight = lax.all_gather(conv_shard, 'sp', axis=0, tiled=True)  68.2 us
    all_gather x1, waiting for transfers between devices, local(): ssd_weight = lax.all_gather(ssd_shard, 'sp', axis=0, tiled=True)  53.7 us
    ppermute x9, waiting for transfers between devices, swapped(): return lax.ppermute(value, axis, [(i, i ^ distance) for i in range(size)])  44 us
    ppermute x9, starting transfers between devices, swapped(): return lax.ppermute(value, axis, [(i, i ^ distance) for i in range(size)])  14.7 us
    unnamed x88, local copies, waits for them, and re-layouts  9.58 us
    dot_general x1, matrix products, local(): jnp.dot(wide_rows, ssd_weight, preferred_element_type=f32).astype(bf16)  8.68 us
    dot_general x2, matrix products, leave(): lax.dot_general(part, exit_weight, (((1,), (1,)), ((), ())), preferred_el...  7.31 us
    dot_general x1, matrix products, local(): jnp.dot(wide_rows, conv_weight[:, :3 * conv_width], preferred_element_typ...  6.02 us
  transfers between devices with their start and end apart: 13, of which 9 were waited for; matrix products, arithmetic and copies ran while one was open for 21% of the time, Pallas kernels for 0%

commit v1 on v0

--- a/solution.py
+++ b/solution.py
@@ -111,7 +111,12 @@
         ],
         axis=1,
     )
-    ssd_weight = lax.all_gather(ssd_shard, "sp", axis=0, tiled=True)
+    ring = [ssd_shard]
+    for hop in range(15):
+        ring.append(lax.ppermute(ring[-1], "sp", [(dev, (dev + 1) % 16) for dev in range(16)]))
+    ssd_weight = jnp.roll(
+        jnp.concatenate(ring[::-1], axis=0), (lax.axis_index("sp") + 1) * ring[0].shape[0], axis=0
+    )
     float_rows = layer_source_rows.astype(f32)
     normed = (
         float_rows

time: 283 us -> 366 us (1.29)
  waiting for transfers between devices: 166 us -> 239 us
  local copies, waits for them, and re-layouts: 29 us -> 49.8 us
  starting transfers between devices: 18.4 us -> 8.21 us
  matrix products: 30.1 us -> 22.5 us
  other arithmetic: 25.2 us -> 31.1 us
    ppermute x0 -> x15, waiting for transfers between devices: none -> 186 us  [local(): lax.ppermute(ring[-1], 'sp', [(dev, (dev + 1) % 16) for dev in range(16)])]
    all_gather x1, waiting for transfers between devices: 68.2 us -> 0.02 us  [local(): conv_weight = lax.all_gather(conv_shard, 'sp', axis=0, tiled=True)]
    all_gather x1 -> x0, waiting for transfers between devices: 53.7 us -> none  [local(): ssd_weight = lax.all_gather(ssd_shard, 'sp', axis=0, tiled=True)]
    unnamed x88 -> x140, local copies, waits for them, and re-layouts: 9.58 us -> 34.2 us
    ppermute x9, starting transfers between devices: 14.7 us -> 5.04 us  [swapped(): return lax.ppermute(value, axis, [(i, i ^ distance) for i in range(size)])]
    ppermute x9, waiting for transfers between devices: 44 us -> 53.1 us  [swapped(): return lax.ppermute(value, axis, [(i, i ^ distance) for i in range(size)])]
    dot_general x2, matrix products: 7.31 us -> 2.87 us  [leave(): lax.dot_general(part, exit_weight, (((1,), (1,)), ((), ())), preferred_el...]
  transfers between devices with their start and end apart: 13 -> 27, of which waited for: 9 -> 21; matrix products, arithmetic and copies ran while one was open for 21% -> 23% of each run, Pallas kernels for 0% -> 0%
where the time goes in v1:
time: 366 us; the launch traced here: 365 us
  waiting for transfers between devices  239 us (65%)
  local copies, waits for them, and re-layouts  49.8 us (14%)
  other arithmetic  31.1 us (8%)
  matrix products  22.5 us (6%)
  between operations  14.6 us (4%)
  starting transfers between devices  8.21 us (2%)
    ppermute x15, waiting for transfers between devices, local(): lax.ppermute(ring[-1], 'sp', [(dev, (dev + 1) % 16) for dev in range(16)])  186 us
    ppermute x9, waiting for transfers between devices, swapped(): return lax.ppermute(value, axis, [(i, i ^ distance) for i in range(size)])  53.1 us
    unnamed x140, local copies, waits for them, and re-layouts  34.2 us
  transfers between devices with their start and end apart: 27, of which 21 were waited for; matrix products, arithmetic and copies ran while one was open for 23% of the time, Pallas kernels for 0%

profile of v1, /device:TPU:0, one launch (start us, length us, event | category | flops | bytes accessed | tf_op | source)
XLA Modules:
  0.0 365.2 jit_solution(15607009707973153050)
XLA Ops:
  9.3 14.7 %collective-permute-done.3 = bf16[128,3072]{1,0:T(8,128)(2,1)S(1)} collective-permute-done((bf16[128,3072]{1,0:T(8,128)(2,1)S(1)}, bf16[128,3072]{1,0:T(8,128)(2,1)S(1)}, u32[]{:S(2)}, u32[]{:S(2)}) %collective-permute-start.3) | collective-permute-done | bytes 786464 | tf_op jit(solution)/shard_map/ppermute | solution.py:116
  23.9 14.1 %collective-permute-done.4 = bf16[128,3072]{1,0:T(8,128)(2,1)S(1)} collective-permute-done((bf16[128,3072]{1,0:T(8,128)(2,1)S(1)}, bf16[128,3072]{1,0:T(8,128)(2,1)S(1)}, u32[]{:S(2)}, u32[]{:S(2)}) %collective-permute-start.4) | collective-permute-done | bytes 786464 | tf_op jit(solution)/shard_map/ppermute | solution.py:116
  39.0 14.1 %collective-permute-done.5 = bf16[128,3072]{1,0:T(8,128)(2,1)S(1)} collective-permute-done((bf16[128,3072]{1,0:T(8,128)(2,1)S(1)}, bf16[128,3072]{1,0:T(8,128)(2,1)S(1)}, u32[]{:S(2)}, u32[]{:S(2)}) %collective-permute-start.5) | collective-permute-done | bytes 786464 | tf_op jit(solution)/shard_map/ppermute | solution.py:116
  54.0 14.1 %collective-permute-done.6 = bf16[128,3072]{1,0:T(8,128)(2,1)S(1)} collective-permute-done((bf16[128,3072]{1,0:T(8,128)(2,1)S(1)}, bf16[128,3072]{1,0:T(8,128)(2,1)S(1)}, u32[]{:S(2)}, u32[]{:S(2)}) %collective-permute-start.6) | collective-permute-done | bytes 786464 | tf_op jit(solution)/shard_map/ppermute | solution.py:116
  69.1 14.1 %collective-permute-done.7 = bf16[128,3072]{1,0:T(8,128)(2,1)S(1)} collective-permute-done((bf16[128,3072]{1,0:T(8,128)(2,1)S(1)}, bf16[128,3072]{1,0:T(8,128)(2,1)S(1)}, u32[]{:S(2)}, u32[]{:S(2)}) %collective-permute-start.7) | collective-permute-done | bytes 786464 | tf_op jit(solution)/shard_map/ppermute | solution.py:116
  84.1 14.1 %collective-permute-done.8 = bf16[128,3072]{1,0:T(8,128)(2,1)S(1)} collective-permute-done((bf16[128,3072]{1,0:T(8,128)(2,1)S(1)}, bf16[128,3072]{1,0:T(8,128)(2,1)S(1)}, u32[]{:S(2)}, u32[]{:S(2)}) %collective-permute-start.8) | collective-permute-done | bytes 786464 | tf_op jit(solution)/shard_map/ppermute | solution.py:116
  99.1 14.2 %collective-permute-done.9 = bf16[128,3072]{1,0:T(8,128)(2,1)} collective-permute-done((bf16[128,3072]{1,0:T(8,128)(2,1)S(1)}, bf16[128,3072]{1,0:T(8,128)(2,1)}, u32[]{:S(2)}, u32[]{:S(2)}) %collective-permute-start.9) | collective-permute-done | bytes 786464 | tf_op jit(solution)/shard_map/ppermute | solution.py:116
  119.1 8.6 %collective-permute-done.10 = bf16[128,3072]{1,0:T(8,128)(2,1)} collective-permute-done((bf16[128,3072]{1,0:T(8,128)(2,1)}, bf16[128,3072]{1,0:T(8,128)(2,1)}, u32[]{:S(2)}, u32[]{:S(2)}) %collective-permute-start.10) | collective-permute-done | bytes 786464 | tf_op jit(solution)/shard_map/ppermute | solution.py:116
  134.9 7.2 %collective-permute-done.11 = bf16[128,3072]{1,0:T(8,128)(2,1)} collective-permute-done((bf16[128,3072]{1,0:T(8,128)(2,1)}, bf16[128,3072]{1,0:T(8,128)(2,1)}, u32[]{:S(2)}, u32[]{:S(2)}) %collective-permute-start.11) | collective-permute-done | bytes 786464 | tf_op jit(solution)/shard_map/ppermute | solution.py:116
  144.8 11.8 %collective-permute-done.12 = bf16[128,3072]{1,0:T(8,128)(2,1)} collective-permute-done((bf16[128,3072]{1,0:T(8,128)(2,1)}, bf16[128,3072]{1,0:T(8,128)(2,1)}, u32[]{:S(2)}, u32[]{:S(2)}) %collective-permute-start.12) | collective-permute-done | bytes 786464 | tf_op jit(solution)/shard_map/ppermute | solution.py:116
  159.7 11.4 %collective-permute-done.13 = bf16[128,3072]{1,0:T(8,128)(2,1)} collective-permute-done((bf16[128,3072]{1,0:T(8,128)(2,1)}, bf16[128,3072]{1,0:T(8,128)(2,1)}, u32[]{:S(2)}, u32[]{:S(2)}) %collective-permute-start.13) | collective-permute-done | bytes 786464 | tf_op jit(solution)/shard_map/ppermute | solution.py:116
  175.0 10.6 %collective-permute-done.14 = bf16[128,3072]{1,0:T(8,128)(2,1)} collective-permute-done((bf16[128,3072]{1,0:T(8,128)(2,1)}, bf16[128,3072]{1,0:T(8,128)(2,1)}, u32[]{:S(2)}, u32[]{:S(2)}) %collective-permute-start.14) | collective-permute-done | bytes 786464 | tf_op jit(solution)/shard_map/ppermute | solution.py:116
  186.3 13.6 %collective-permute-done.15 = bf16[128,3072]{1,0:T(8,128)(2,1)S(1)} collective-permute-done((bf16[128,3072]{1,0:T(8,128)(2,1)}, bf16[128,3072]{1,0:T(8,128)(2,1)S(1)}, u32[]{:S(2)}, u32[]{:S(2)}) %collective-permute-start.15) | collective-permute-done | bytes 786464 | tf_op jit(solution)/shard_map/ppermute | solution.py:116
  204.1 10.8 %collective-permute-done.16 = bf16[128,3072]{1,0:T(8,128)(2,1)} collective-permute-done((bf16[128,3072]{1,0:T(8,128)(2,1)S(1)}, bf16[128,3072]{1,0:T(8,128)(2,1)}, u32[]{:S(2)}, u32[]{:S(2)}) %collective-permute-start.16) | collective-permute-done | bytes 786464 | tf_op jit(solution)/shard_map/ppermute | solution.py:116
  217.0 12.4 %collective-permute-done.17 = bf16[128,3072]{1,0:T(8,128)(2,1)} collective-permute-done((bf16[128,3072]{1,0:T(8,128)(2,1)}, bf16[128,3072]{1,0:T(8,128)(2,1)}, u32[]{:S(2)}, u32[]{:S(2)}) %collective-permute-start.17) | collective-permute-done | bytes 786464 | tf_op jit(solution)/shard_map/ppermute | solution.py:116
  249.9 5.6 %fusion.4 = bf16[400,3072]{1,0:T(8,128)(2,1)S(1)} fusion(bf16[400,2048]{1,0:T(8,128)(2,1)S(1)} %constant_dynamic-update-slice_fusion, bf16[4096,3072]{1,0:T(8,128)(2,1)S(1)} %constant_dynamic-update-slice_fusion.3, s32[]{:T(128)S(6)} %select_n.84), kind=kOutput, calls=%fused_computation.4 | convolution fusion | flops 5034393600 | bytes 16678916 | tf_op jit(solution)/shard_map/dot_general | solution.py:163
  255.5 3.2 multiply_convert_fusion
  273.8 12.4 %collective-permute-done.21 = f32[2,8]{1,0:T(2,128)S(1)} collective-permute-done((f32[2,8]{1,0:T(2,128)S(1)}, f32[2,8]{1,0:T(2,128)S(1)}, u32[]{:S(2)}, u32[]{:S(2)}) %collective-permute-start.21) | collective-permute-done | bytes 96 | tf_op jit(solution)/shard_map/ppermute | solution.py:15
  286.3 3.5 collective-permute-done.23
  299.9 9.8 %collective-permute-done.22 = bf16[8,2,64,128]{3,2,1,0:T(8,128)(2,1)} collective-permute-done((bf16[8,2,64,128]{3,2,1,0:T(8,128)(2,1)}, bf16[8,2,64,128]{3,2,1,0:T(8,128)(2,1)}, u32[]{:S(2)}, u32[]{:S(2)}) %collective-permute-start.22) | collective-permute-done | bytes 262176 | tf_op jit(solution)/shard_map/ppermute | solution.py:15
  311.5 8.6 %collective-permute-done.24 = bf16[8,64,128]{2,1,0:T(8,128)(2,1)S(1)} collective-permute-done((bf16[8,64,128]{2,1,0:T(8,128)(2,1)S(1)}, bf16[8,64,128]{2,1,0:T(8,128)(2,1)S(1)}, u32[]{:S(2)}, u32[]{:S(2)}) %collective-permute-start.24) | collective-permute-done | bytes 131104 | tf_op jit(solution)/shard_map/ppermute | solution.py:15
  323.9 4.1 %multiply_reduce_fusion = (f32[8,3,128]{2,1,0:T(4,128)S(1)}, f32[8,3,128,64]{2,3,1,0:T(8,128)S(1)}) fusion(f32[3,128,8,64]{1,3,0,2:T(8,128)} %copy.135, f32[8,3,128]{2,1,0:T(4,128)S(1)} %copy.133, f32[8,3,128,128]{2,3,1,0:T(8,128)} %fusion.54, f32[8,3,128]{2,1,0:T(4,128)S(1)} %copy.132, bf16[3,128,8,64]{1,3,0,2:T(8,128)(2,1)S(1)} %copy-done.18, ...), kind=kOutput, calls=%fused_computation.75 | convolution fusion | flops 156693504 | bytes 8351744 | tf_op jit(solution)/shard_map/hbts,hbsp->hbtp/dot_general | solution.py:196
  329.2 6.2 %fusion.11 = bf16[400,1536]{1,0:T(8,128)(2,1)S(1)} fusion(bf16[400,2048]{1,0:T(8,128)(2,1)} %copy-done.46, bf16[2048,2560]{0,1:T(8,128)(2,1)} %all-gather.2.cloned.1.call-done), kind=kOutput, calls=%fused_computation.10 | convolution fusion | flops 2517196800 | bytes 9158656 | tf_op jit(solution)/shard_map/dot_general | solution.py:210
  337.8 18.6 %collective-permute-done.25 = bf16[192,2048]{1,0:T(8,128)(2,1)S(1)} collective-permute-done((bf16[192,2048]{1,0:T(8,128)(2,1)S(1)}, bf16[192,2048]{1,0:T(8,128)(2,1)S(1)}, u32[]{:S(2)}, u32[]{:S(2)}) %collective-permute-start.25) | collective-permute-done | bytes 786464 | tf_op jit(solution)/shard_map/ppermute | solution.py:15
  (277 shorter events, 92.9 us)
Async XLA Ops:
  6.5 322.7 %all-gather.2.cloned.1.call-start = ((), (), s32[]{:S(2)}) async-start(), calls=%async_computation | async-start | bytes 11141120 | tf_op jit(solution)/shard_map/all_gather | solution.py:133
  8.7 15.2 %collective-permute-start.3 = (bf16[128,3072]{1,0:T(8,128)(2,1)S(1)}, bf16[128,3072]{1,0:T(8,128)(2,1)S(1)}, u32[]{:S(2)}, u32[]{:S(2)}) collective-permute-start(bf16[128,3072]{1,0:T(8,128)(2,1)S(1)} %pad_maximum_fusion.1), channel_id=1, source_target_pairs={{0,2},{2,4},{4,6},{6,8},{8,10},{10,12},{12,14},{14,16},{16,18},{18... | collective-permute-start | bytes 2359304 | tf_op jit(solution)/shard_map/ppermute | solution.py:116
  23.9 14.1 %collective-permute-start.4 = (bf16[128,3072]{1,0:T(8,128)(2,1)S(1)}, bf16[128,3072]{1,0:T(8,128)(2,1)S(1)}, u32[]{:S(2)}, u32[]{:S(2)}) collective-permute-start(bf16[128,3072]{1,0:T(8,128)(2,1)S(1)} %collective-permute-done.3), channel_id=1, source_target_pairs={{0,2},{2,4},{4,6},{6,8},{8,10},{10,12},{12,14},{14,16},{16,18},{18... | collective-permute-start | bytes 2359304 | tf_op jit(solution)/shard_map/ppermute | solution.py:116
  38.9 14.1 %collective-permute-start.5 = (bf16[128,3072]{1,0:T(8,128)(2,1)S(1)}, bf16[128,3072]{1,0:T(8,128)(2,1)S(1)}, u32[]{:S(2)}, u32[]{:S(2)}) collective-permute-start(bf16[128,3072]{1,0:T(8,128)(2,1)S(1)} %collective-permute-done.4), channel_id=1, source_target_pairs={{0,2},{2,4},{4,6},{6,8},{8,10},{10,12},{12,14},{14,16},{16,18},{18... | collective-permute-start | bytes 2359304 | tf_op jit(solution)/shard_map/ppermute | solution.py:116
  54.0 14.1 %collective-permute-start.6 = (bf16[128,3072]{1,0:T(8,128)(2,1)S(1)}, bf16[128,3072]{1,0:T(8,128)(2,1)S(1)}, u32[]{:S(2)}, u32[]{:S(2)}) collective-permute-start(bf16[128,3072]{1,0:T(8,128)(2,1)S(1)} %collective-permute-done.5), channel_id=1, source_target_pairs={{0,2},{2,4},{4,6},{6,8},{8,10},{10,12},{12,14},{14,16},{16,18},{18... | collective-permute-start | bytes 2359304 | tf_op jit(solution)/shard_map/ppermute | solution.py:116
  69.1 14.1 %collective-permute-start.7 = (bf16[128,3072]{1,0:T(8,128)(2,1)S(1)}, bf16[128,3072]{1,0:T(8,128)(2,1)S(1)}, u32[]{:S(2)}, u32[]{:S(2)}) collective-permute-start(bf16[128,3072]{1,0:T(8,128)(2,1)S(1)} %collective-permute-done.6), channel_id=1, source_target_pairs={{0,2},{2,4},{4,6},{6,8},{8,10},{10,12},{12,14},{14,16},{16,18},{18... | collective-permute-start | bytes 2359304 | tf_op jit(solution)/shard_map/ppermute | solution.py:116
  84.1 14.1 %collective-permute-start.8 = (bf16[128,3072]{1,0:T(8,128)(2,1)S(1)}, bf16[128,3072]{1,0:T(8,128)(2,1)S(1)}, u32[]{:S(2)}, u32[]{:S(2)}) collective-permute-start(bf16[128,3072]{1,0:T(8,128)(2,1)S(1)} %collective-permute-done.7), channel_id=1, source_target_pairs={{0,2},{2,4},{4,6},{6,8},{8,10},{10,12},{12,14},{14,16},{16,18},{18... | collective-permute-start | bytes 2359304 | tf_op jit(solution)/shard_map/ppermute | solution.py:116
  99.1 14.2 %collective-permute-start.9 = (bf16[128,3072]{1,0:T(8,128)(2,1)S(1)}, bf16[128,3072]{1,0:T(8,128)(2,1)}, u32[]{:S(2)}, u32[]{:S(2)}) collective-permute-start(bf16[128,3072]{1,0:T(8,128)(2,1)S(1)} %collective-permute-done.8), channel_id=1, source_target_pairs={{0,2},{2,4},{4,6},{6,8},{8,10},{10,12},{12,14},{14,16},{16,18},{18... | collective-permute-start | bytes 2359304 | tf_op jit(solution)/shard_map/ppermute | solution.py:116
  113.3 14.4 %collective-permute-start.10 = (bf16[128,3072]{1,0:T(8,128)(2,1)}, bf16[128,3072]{1,0:T(8,128)(2,1)}, u32[]{:S(2)}, u32[]{:S(2)}) collective-permute-start(bf16[128,3072]{1,0:T(8,128)(2,1)} %collective-permute-done.9), channel_id=1, source_target_pairs={{0,2},{2,4},{4,6},{6,8},{8,10},{10,12},{12,14},{14,16},{16,18},{18... | collective-permute-start | bytes 2359304 | tf_op jit(solution)/shard_map/ppermute | solution.py:116
  117.2 40.7 %collective-permute-start = (bf16[192,2048]{1,0:T(8,128)(2,1)}, bf16[192,2048]{1,0:T(8,128)(2,1)}, u32[]{:S(2)}, u32[]{:S(2)}) collective-permute-start(bf16[192,2048]{1,0:T(8,128)(2,1)} %get-tuple-element.25), channel_id=1, source_target_pairs={{0,1},{1,0},{2,3},{3,2},{4,5},{5,4},{6,7},{7,6},{8,9},{9,8},{10,11... | collective-permute-start | bytes 2359304 | tf_op jit(solution)/shard_map/ppermute | solution.py:15
  127.7 14.4 %collective-permute-start.11 = (bf16[128,3072]{1,0:T(8,128)(2,1)}, bf16[128,3072]{1,0:T(8,128)(2,1)}, u32[]{:S(2)}, u32[]{:S(2)}) collective-permute-start(bf16[128,3072]{1,0:T(8,128)(2,1)} %collective-permute-done.10), channel_id=1, source_target_pairs={{0,2},{2,4},{4,6},{6,8},{8,10},{10,12},{12,14},{14,16},{16,18},{18... | collective-permute-start | bytes 2359304 | tf_op jit(solution)/shard_map/ppermute | solution.py:116
  142.2 14.4 %collective-permute-start.12 = (bf16[128,3072]{1,0:T(8,128)(2,1)}, bf16[128,3072]{1,0:T(8,128)(2,1)}, u32[]{:S(2)}, u32[]{:S(2)}) collective-permute-start(bf16[128,3072]{1,0:T(8,128)(2,1)} %collective-permute-done.11), channel_id=1, source_target_pairs={{0,2},{2,4},{4,6},{6,8},{8,10},{10,12},{12,14},{14,16},{16,18},{18... | collective-permute-start | bytes 2359304 | tf_op jit(solution)/shard_map/ppermute | solution.py:116
  156.6 14.5 %collective-permute-start.13 = (bf16[128,3072]{1,0:T(8,128)(2,1)}, bf16[128,3072]{1,0:T(8,128)(2,1)}, u32[]{:S(2)}, u32[]{:S(2)}) collective-permute-start(bf16[128,3072]{1,0:T(8,128)(2,1)} %collective-permute-done.12), channel_id=1, source_target_pairs={{0,2},{2,4},{4,6},{6,8},{8,10},{10,12},{12,14},{14,16},{16,18},{18... | collective-permute-start | bytes 2359304 | tf_op jit(solution)/shard_map/ppermute | solution.py:116
  171.1 14.4 %collective-permute-start.14 = (bf16[128,3072]{1,0:T(8,128)(2,1)}, bf16[128,3072]{1,0:T(8,128)(2,1)}, u32[]{:S(2)}, u32[]{:S(2)}) collective-permute-start(bf16[128,3072]{1,0:T(8,128)(2,1)} %collective-permute-done.13), channel_id=1, source_target_pairs={{0,2},{2,4},{4,6},{6,8},{8,10},{10,12},{12,14},{14,16},{16,18},{18... | collective-permute-start | bytes 2359304 | tf_op jit(solution)/shard_map/ppermute | solution.py:116
  172.4 44.5 %collective-permute-start.1 = (bf16[8,2048]{1,0:T(8,128)(2,1)S(1)}, bf16[8,2048]{1,0:T(8,128)(2,1)S(1)}, u32[]{:S(2)}, u32[]{:S(2)}) collective-permute-start(bf16[8,2048]{1,0:T(8,128)(2,1)S(1)} %get-tuple-element.32), channel_id=1, source_target_pairs={{0,2},{2,4},{4,6},{6,8},{8,10},{10,12},{12,14},{14,16},{16,18},{18... | collective-permute-start | bytes 98312 | tf_op jit(solution)/shard_map/ppermute | solution.py:33
  173.7 43.3 %collective-permute-start.2 = (bf16[8,2048]{1,0:T(8,128)(2,1)S(1)}, bf16[8,2048]{1,0:T(8,128)(2,1)S(1)}, u32[]{:S(2)}, u32[]{:S(2)}) collective-permute-start(bf16[8,2048]{1,0:T(8,128)(2,1)S(1)} %get-tuple-element.31), channel_id=1, source_target_pairs={{2,0},{4,2},{6,4},{8,6},{10,8},{12,10},{14,12},{16,14},{18,16},{20... | collective-permute-start | bytes 98312 | tf_op jit(solution)/shard_map/ppermute | solution.py:34
  185.5 14.3 %collective-permute-start.15 = (bf16[128,3072]{1,0:T(8,128)(2,1)}, bf16[128,3072]{1,0:T(8,128)(2,1)S(1)}, u32[]{:S(2)}, u32[]{:S(2)}) collective-permute-start(bf16[128,3072]{1,0:T(8,128)(2,1)} %collective-permute-done.14), channel_id=1, source_target_pairs={{0,2},{2,4},{4,6},{6,8},{8,10},{10,12},{12,14},{14,16},{16,18},{18... | collective-permute-start | bytes 2359304 | tf_op jit(solution)/shard_map/ppermute | solution.py:116
  200.7 14.2 %collective-permute-start.16 = (bf16[128,3072]{1,0:T(8,128)(2,1)S(1)}, bf16[128,3072]{1,0:T(8,128)(2,1)}, u32[]{:S(2)}, u32[]{:S(2)}) collective-permute-start(bf16[128,3072]{1,0:T(8,128)(2,1)S(1)} %collective-permute-done.15), channel_id=1, source_target_pairs={{0,2},{2,4},{4,6},{6,8},{8,10},{10,12},{12,14},{14,16},{16,18},{18... | collective-permute-start | bytes 2359304 | tf_op jit(solution)/shard_map/ppermute | solution.py:116
  215.0 14.4 %collective-permute-start.17 = (bf16[128,3072]{1,0:T(8,128)(2,1)}, bf16[128,3072]{1,0:T(8,128)(2,1)}, u32[]{:S(2)}, u32[]{:S(2)}) collective-permute-start(bf16[128,3072]{1,0:T(8,128)(2,1)} %collective-permute-done.16), channel_id=1, source_target_pairs={{0,2},{2,4},{4,6},{6,8},{8,10},{10,12},{12,14},{14,16},{16,18},{18... | collective-permute-start | bytes 2359304 | tf_op jit(solution)/shard_map/ppermute | solution.py:116
  216.2 52.3 %collective-permute-start.19 = (f32[2,8]{1,0:T(2,128)}, f32[2,8]{1,0:T(2,128)}, u32[]{:S(2)}, u32[]{:S(2)}) collective-permute-start(f32[2,8]{1,0:T(2,128)} %exp.52), channel_id=1, source_target_pairs={{0,2},{2,0},{4,6},{6,4},{8,10},{10,8},{12,14},{14,12},{16,18},{18,... | collective-permute-start | bytes 200 | tf_op jit(solution)/shard_map/ppermute | solution.py:15
  271.2 19.7 %collective-permute-start.20 = (bf16[8,2,64,128]{3,2,1,0:T(8,128)(2,1)}, bf16[8,2,64,128]{3,2,1,0:T(8,128)(2,1)}, u32[]{:S(2)}, u32[]{:S(2)}) collective-permute-start(bf16[8,2,64,128]{3,2,1,0:T(8,128)(2,1)} %fusion.124), channel_id=1, source_target_pairs={{0,4},{2,6},{4,0},{6,2},{8,12},{10,14},{12,8},{14,10},{16,20},{18,... | collective-permute-start | bytes 786440 | tf_op jit(solution)/shard_map/ppermute | solution.py:15
  271.6 14.6 %collective-permute-start.21 = (f32[2,8]{1,0:T(2,128)S(1)}, f32[2,8]{1,0:T(2,128)S(1)}, u32[]{:S(2)}, u32[]{:S(2)}) collective-permute-start(f32[2,8]{1,0:T(2,128)S(1)} %get-tuple-element.64), channel_id=1, source_target_pairs={{0,4},{2,6},{4,0},{6,2},{8,12},{10,14},{12,8},{14,10},{16,20},{18,... | collective-permute-start | bytes 200 | tf_op jit(solution)/shard_map/ppermute | solution.py:15
  293.0 16.7 %collective-permute-start.22 = (bf16[8,2,64,128]{3,2,1,0:T(8,128)(2,1)}, bf16[8,2,64,128]{3,2,1,0:T(8,128)(2,1)}, u32[]{:S(2)}, u32[]{:S(2)}) collective-permute-start(bf16[8,2,64,128]{3,2,1,0:T(8,128)(2,1)} %fusion.95), channel_id=1, source_target_pairs={{0,8},{2,10},{4,12},{6,14},{8,0},{10,2},{12,4},{14,6},{16,24},{18,... | collective-permute-start | bytes 786440 | tf_op jit(solution)/shard_map/ppermute | solution.py:15
  336.9 19.6 %collective-permute-start.25 = (bf16[192,2048]{1,0:T(8,128)(2,1)S(1)}, bf16[192,2048]{1,0:T(8,128)(2,1)S(1)}, u32[]{:S(2)}, u32[]{:S(2)}) collective-permute-start(bf16[192,2048]{1,0:T(8,128)(2,1)S(1)} %fusion.20), channel_id=1, source_target_pairs={{0,1},{1,0},{2,3},{3,2},{4,5},{5,4},{6,7},{7,6},{8,9},{9,8},{10,11... | collective-permute-start | bytes 2359304 | tf_op jit(solution)/shard_map/ppermute | solution.py:15
  (53 other events, 1009.8 us)
Sparse Core Ops, SparseCore 0:
  217.0 97.4 all-gather.1
